TPU v7x, 32 devices: a whole 2x2x4 slice. The times are simulated.
32 devices in a mesh: grp: 2 (over y), sp: 4 (over z), tp: 4 (over x, core).
Axes of the slice: x: 2, y: 2, z: 4, core: 2. Of those that a mesh axis runs over, the one named last changes fastest.
Arguments:
- hidden_in: bfloat16 [3072, 4096], P(('grp', 'sp'), 'tp'), parts along dimension 0, may hold values from -30 to 30
- in_gain: float32 [2, 4096], P(None, 'tp'), may hold values from 0.1 to 1.9
- w_value: bfloat16 [2, 4096, 2048], P(None, 'sp', 'tp'), may hold values from -0.09375 to 0.09375
- w_gate: bfloat16 [2, 4096, 2048], P(None, 'sp', 'tp'), may hold values from -0.09375 to 0.09375
- conv_taps: float32 [2, 31, 2048], P(None, None, 'tp'), may hold values from -9 to 9
- norm_gain: float32 [2, 2048], P(None, 'tp'), may hold values from 0.1 to 1.9
- norm_shift: float32 [2, 2048], P(None, 'tp'), may hold values from -3 to 3
- w_out: bfloat16 [2, 2048, 4096], P(None, 'tp', 'sp'), may hold values from -0.125 to 0.125
Outputs:
- hidden_out: bfloat16 [3072, 4096], P(('grp', 'sp'), 'tp'), parts along dimension 0
There are 2 independent parts, one for each index of `grp`. A program takes and returns all parts, laid end to end along the dimension named above; an argument that names none is the same for every part. Nothing has to cross between parts.
All inputs are finite; a program needn't handle non-finite values.
Results may differ from a plain program's by a relative error of at most 0.013.
Values may be sent and summed in bfloat16 or wider, within the bound.
A program may use at most 64 MiB of HBM per device.

v0:
```python
import jax
import jax.numpy as jnp
from jax import lax
from jax.sharding import PartitionSpec as P

D = 4096
C = 2048
epsilon = 1e-06


def passed_along(value, axis, steps):
    count = lax.axis_size(axis)
    initial, last = (max(0, -steps), min(count, count - steps))
    return lax.ppermute(value, axis, [(source, source + steps) for source in range(initial, last)])


def depthwise(extended, kernel_taps):
    conved = lax.conv_general_dilated(
        extended.astype(jnp.float32)[None],
        kernel_taps[:, None, :],
        (1,),
        [(0, 0)],
        dimension_numbers=("NWC", "WIO", "NWC"),
        feature_group_count=extended.shape[1],
        precision=lax.Precision.HIGHEST,
    )
    return conved[0]


def shards(hidden_in, in_gain, w_value, w_gate, conv_taps, norm_gain, norm_shift, w_out):
    layer_count = w_value.shape[0]
    reach_rows = conv_taps.shape[1] - 1
    value_all, gate_all = (
        lax.all_gather(w_value, "sp", axis=1, tiled=True),
        lax.all_gather(w_gate, "sp", axis=1, tiled=True),
    )
    out_all = lax.all_gather(w_out, "sp", axis=2, tiled=True)
    current = hidden_in
    for layer_idx in range(layer_count):
        widened = current.astype(jnp.float32)
        squares = lax.psum(jnp.sum(widened * widened, axis=1), "tp")
        normalized = (
            widened * lax.rsqrt(squares / D + epsilon)[:, None] * in_gain[layer_idx]
        ).astype(jnp.bfloat16)
        gathered = lax.all_gather(normalized, "tp", axis=1, tiled=True)
        value_part = jnp.dot(gathered, value_all[layer_idx], preferred_element_type=jnp.float32)
        gate_part = jnp.dot(gathered, gate_all[layer_idx], preferred_element_type=jnp.float32)
        gated = (value_part * jax.nn.sigmoid(gate_part)).astype(jnp.bfloat16)
        before = passed_along(gated[gated.shape[0] - reach_rows :], "sp", 1)
        extended = jnp.concatenate([before, gated], axis=0)
        residual = current
        conved = depthwise(extended, conv_taps[layer_idx])
        total_sum, total_squares = lax.psum(
            (jnp.sum(conved, axis=1), jnp.sum(conved * conved, axis=1)), "tp"
        )
        row_mean = total_sum / C
        spread = total_squares / C - row_mean * row_mean
        normed = (conved - row_mean[:, None]) * lax.rsqrt(spread + epsilon)[:, None] * norm_gain[
            layer_idx
        ] + norm_shift[layer_idx]
        mixed_out = jax.nn.silu(normed).astype(jnp.bfloat16)
        partial_value = jnp.dot(mixed_out, out_all[layer_idx], preferred_element_type=jnp.float32)
        summed = lax.psum_scatter(
            partial_value.astype(jnp.bfloat16), "tp", scatter_dimension=1, tiled=True
        ).astype(jnp.float32)
        current = (residual.astype(jnp.float32) + summed).astype(jnp.bfloat16)
    return current


def solution(mesh):
    placed = (
        P(("grp", "sp"), "tp"),
        P(None, "tp"),
        P(None, "sp", "tp"),
        P(None, "sp", "tp"),
        P(None, None, "tp"),
        P(None, "tp"),
        P(None, "tp"),
        P(None, "tp", "sp"),
    )
    return jax.shard_map(
        shards, mesh=mesh, in_specs=placed, out_specs=P(("grp", "sp"), "tp"), check_vma=False
    )
```

profile of v0, /device:TPU:0, one launch (start us, length us, event | category | flops | bytes accessed | tf_op | source)
XLA Modules:
  0.0 657.1 jit_solution(9422213232833642842)
XLA Ops:
  6.5 1.4 fusion.4
  7.9 8.4 %psum.42 = f32[384]{0:T(512)S(1)} all-reduce(f32[384]{0:T(512)S(1)} %fusion.4), channel_id=1, replica_groups=mesh['grp'=2,'sp'=4,'tp'=4] {'tp'}, use_global_device_ids=true, to_apply=%region_1.0 | all-reduce | flops 384 | bytes 3072 | tf_op jit(solution)/shard_map/psum | solution.py:41
  16.3 0.8 fusion.62
  17.1 2.3 fusion.6
  19.4 0.7 all-gather.10.cloned.1.call-update
  20.2 0.7 all-gather.8.cloned.1.call-update
  20.9 0.5 all-gather.12.cloned.1.call-update
  21.5 26.8 %all-gather.6.cloned.1.call-done = bf16[384,4096]{1,0:T(8,128)(2,1)} async-done(((bf16[384,1024]{1,0:T(8,128)(2,1)}), bf16[384,4096]{1,0:T(8,128)(2,1)}) %all-gather.6.cloned.1.call-update) | async-done | bytes 3145744 | tf_op jit(solution)/shard_map/all_gather | solution.py:45
  48.3 151.2 %all-gather.10.cloned.1.call-done = bf16[2,4096,512]{2,1,0:T(8,128)(2,1)} async-done(((bf16[2,1024,512]{2,1,0:T(8,128)(2,1)}), bf16[2,4096,512]{2,1,0:T(8,128)(2,1)}) %all-gather.10.cloned.1.call-update) | async-done | bytes 8388624 | tf_op jit(solution)/shard_map/all_gather | solution.py:35
  199.5 5.9 fusion.23
  205.5 143.5 %all-gather.8.cloned.1.call-done = bf16[2,4096,512]{2,1,0:T(8,128)(2,1)} async-done(((bf16[2,1024,512]{2,1,0:T(8,128)(2,1)}), bf16[2,4096,512]{2,1,0:T(8,128)(2,1)}) %all-gather.8.cloned.1.call-update) | async-done | bytes 8388624 | tf_op jit(solution)/shard_map/all_gather | solution.py:34
  349.0 4.2 fusion.25
  353.2 1.4 collective-permute-start
  354.6 1.6 collective-permute-done
  356.2 0.1 maximum_bitcast_fusion
  356.4 0.1 copy.14
  356.6 1.9 fusion.65
  358.5 0.5 copy.16
  359.0 0.1 reshape.62
  359.1 0.5 copy.15
  359.6 0.1 reshape.60
  359.7 0.2 slice_reduce_fusion.1
  359.9 6.6 all-reduce.1
  366.5 131.7 %all-gather.12.cloned.1.call-done = bf16[2,512,4096]{2,1,0:T(8,128)(2,1)} async-done(((bf16[2,512,1024]{2,1,0:T(8,128)(2,1)}), bf16[2,512,4096]{2,1,0:T(8,128)(2,1)}) %all-gather.12.cloned.1.call-update) | async-done | bytes 8388624 | tf_op jit(solution)/shard_map/all_gather | solution.py:37
  498.2 5.9 convolution_convert_fusion.1
  504.2 36.0 %reduce-scatter.3.cloned.1.call-done = bf16[384,1024]{1,0:T(8,128)(2,1)} async-done(((bf16[384,4096]{1,0:T(8,128)(2,1)}), bf16[384,1024]{1,0:T(8,128)(2,1)}) %reduce-scatter.3.cloned.1.call-update) | async-done | bytes 786448 | tf_op jit(solution)/shard_map/reduce_scatter | solution.py:63
  540.2 1.5 fusion.8
  541.6 5.8 psum.45
  547.4 2.3 fusion.10
  549.8 0.2 reduce-scatter.5.cloned.1.call-start
  550.0 29.1 %all-gather.14.cloned.1.call-done = bf16[384,4096]{1,0:T(8,128)(2,1)} async-done(((bf16[384,1024]{1,0:T(8,128)(2,1)}), bf16[384,4096]{1,0:T(8,128)(2,1)}) %all-gather.14.cloned.1.call-update) | async-done | bytes 3145744 | tf_op jit(solution)/shard_map/all_gather | solution.py:45
  579.0 5.2 fusion.21
  584.2 4.0 fusion.24
  588.3 3.4 collective-permute-start.1
  591.7 1.6 collective-permute-done.1
  593.3 0.1 maximum_bitcast_fusion.1
  593.5 0.1 copy.18
  593.7 2.0 fusion.66
  595.7 0.5 copy.20
  596.2 0.1 reshape.71
  596.3 0.1 slice_reduce_fusion
  596.5 0.5 copy.19
  597.0 0.1 reshape.69
  597.1 0.1 slice_reduce_fusion.2
  597.2 5.9 all-reduce
  603.2 5.9 convolution_convert_fusion
  609.1 38.7 %reduce-scatter.5.cloned.1.call-done = bf16[384,1024]{1,0:T(8,128)(2,1)} async-done(((bf16[384,4096]{1,0:T(8,128)(2,1)}), bf16[384,1024]{1,0:T(8,128)(2,1)}) %reduce-scatter.5.cloned.1.call-update) | async-done | bytes 786448 | tf_op jit(solution)/shard_map/reduce_scatter | solution.py:63
  647.8 2.4 fusion.11
  (40 shorter events, 0.7 us)
Async XLA Ops:
  6.5 41.8 %all-gather.6.cloned.1.call-start = ((), (), s32[]{:S(2)}) async-start(), calls=%async_computation.2 | async-start | bytes 3932160 | tf_op jit(solution)/shard_map/all_gather | solution.py:45
  19.4 2.1 copy-start.2
  19.4 180.2 %all-gather.10.cloned.1.call-start = ((), (), s32[]{:S(2)}) async-start(), calls=%async_computation.4 | async-start | bytes 10485760 | tf_op jit(solution)/shard_map/all_gather | solution.py:35
  20.1 328.8 %all-gather.8.cloned.1.call-start = ((), (), s32[]{:S(2)}) async-start(), calls=%async_computation.3 | async-start | bytes 10485760 | tf_op jit(solution)/shard_map/all_gather | solution.py:34
  20.9 477.4 %all-gather.12.cloned.1.call-start = ((), (), s32[]{:S(2)}) async-start(), calls=%async_computation.5 | async-start | bytes 10485760 | tf_op jit(solution)/shard_map/all_gather | solution.py:37
  21.4 518.8 %reduce-scatter.3.cloned.1.call-start = ((), (), s32[]{:S(2)}) async-start(), calls=%async_computation.6 | async-start | bytes 3932160 | tf_op jit(solution)/shard_map/reduce_scatter | solution.py:63
  48.3 300.6 %copy-start.4 = (bf16[384,4096]{1,0:T(8,128)(2,1)S(1)}, bf16[384,4096]{1,0:T(8,128)(2,1)}, u32[]{:S(2)}) copy-start(bf16[384,4096]{1,0:T(8,128)(2,1)} %all-gather.6.cloned.1.call-done) | copy-start | bytes 9437188
  205.5 149.1 %copy-start.3 = (f32[2,512]{1,0:T(2,128)S(1)}, f32[2,512]{1,0:T(2,128)}, u32[]{:S(2)}) copy-start(f32[2,512]{1,0:T(2,128)} %param.14) | copy-start | bytes 12292
  353.1 3.5 copy-start.6
  353.2 3.5 copy-start.7
  353.2 3.0 collective-permute-start
  504.1 36.1 %copy-start = (bf16[384,1024]{1,0:T(8,128)(2,1)S(1)}, bf16[384,1024]{1,0:T(8,128)(2,1)}, u32[]{:S(2)}) copy-start(bf16[384,1024]{1,0:T(8,128)(2,1)} %param.8) | copy-start | bytes 2359300
  504.1 74.9 %all-gather.14.cloned.1.call-start = ((), (), s32[]{:S(2)}) async-start(), calls=%async_computation.7 | async-start | bytes 3932160 | tf_op jit(solution)/shard_map/all_gather | solution.py:45
  549.8 98.0 %reduce-scatter.5.cloned.1.call-start = ((), (), s32[]{:S(2)}) async-start(), calls=%async_computation.8 | async-start | bytes 3932160 | tf_op jit(solution)/shard_map/reduce_scatter | solution.py:63
  579.0 5.2 copy-start.5
  588.3 5.0 collective-permute-start.1
  609.1 38.7 %copy-start.1 = (bf16[384,1024]{1,0:T(8,128)(2,1)S(1)}, bf16[384,1024]{1,0:T(8,128)(2,1)}, u32[]{:S(2)}) copy-start(bf16[384,1024]{1,0:T(8,128)(2,1)} %reduce-scatter.3.cloned.1.call-done) | copy-start | bytes 2359300
Sparse Core Ops, SparseCore 0:
  19.5 28.8 all-gather.5
  49.9 149.6 all-gather.9
  201.1 147.7 all-gather.7
  350.4 147.7 all-gather.11
  504.2 35.8 reduce-scatter.2
  549.9 29.1 all-gather.13
  609.2 38.5 reduce-scatter.4
where the time goes:
time: 658 us; the launch traced here: 657 us
  waiting for transfers between devices  562 us (85%)
  matrix products  35 us (5%)
  blocking collectives  26.6 us (4%)
  between operations  13.8 us (2%)
  other arithmetic  10.6 us (2%)
    all_gather x1, waiting for transfers between devices, shards(): lax.all_gather(w_gate, 'sp', axis=1, tiled=True)  151 us
    all_gather x1, waiting for transfers between devices, shards(): lax.all_gather(w_value, 'sp', axis=1, tiled=True)  143 us
    all_gather x1, waiting for transfers between devices, shards(): out_all = lax.all_gather(w_out, 'sp', axis=2, tiled=True)  132 us
    reduce_scatter x2, waiting for transfers between devices, shards(): lax.psum_scatter(partial_value.astype(jnp.bfloat16), 'tp', scatter_dimens...  74.7 us
    all_gather x2, waiting for transfers between devices, shards(): gathered = lax.all_gather(normalized, 'tp', axis=1, tiled=True)  55.9 us
    psum x2, blocking collectives, shards(): squares = lax.psum(jnp.sum(widened * widened, axis=1), 'tp')  14.1 us
  transfers between devices with their start and end apart: 9, of which 9 were waited for; matrix products, arithmetic and copies ran while one was open for 2% of the time, Pallas kernels for 0%

commit v1 on v0

--- a/solution.py
+++ b/solution.py
@@ -6,6 +6,21 @@
 D = 4096
 C = 2048
 epsilon = 1e-06
+
+
+def connect_sizes(page):
+    windows = [page]
+    sides = lax.psum(1, axis_name="tp")
+    for hop_no in range(sides - 1):
+        windows.append(
+            lax.ppermute(
+                windows[-1], axis_name="tp", perm=[(rr, (rr + 1) % sides) for rr in range(sides)]
+            )
+        )
+    upper = jnp.roll(
+        jnp.concatenate(windows[::-1], 1), (lax.axis_index("tp") + 1) * page.shape[1], 1
+    )
+    return upper
 
 
 def passed_along(value, axis, steps):
@@ -42,7 +57,7 @@
         normalized = (
             widened * lax.rsqrt(squares / D + epsilon)[:, None] * in_gain[layer_idx]
         ).astype(jnp.bfloat16)
-        gathered = lax.all_gather(normalized, "tp", axis=1, tiled=True)
+        gathered = connect_sizes(normalized)
         value_part = jnp.dot(gathered, value_all[layer_idx], preferred_element_type=jnp.float32)
         gate_part = jnp.dot(gathered, gate_all[layer_idx], preferred_element_type=jnp.float32)
         gated = (value_part * jax.nn.sigmoid(gate_part)).astype(jnp.bfloat16)

time: 658 us -> 626 us (0.951)
  waiting for transfers between devices: 562 us -> 526 us
  other arithmetic: 10.6 us -> 19.1 us
    ppermute x0 -> x6, waiting for transfers between devices: none -> 68.5 us  [connect_sizes(): lax.ppermute(windows[-1], axis_name='tp', perm=[(rr, (rr + 1) % sides) fo...]
    all_gather x2 -> x0, waiting for transfers between devices: 55.9 us -> none  [shards(): gathered = lax.all_gather(normalized, 'tp', axis=1, tiled=True)]
    all_gather x1, waiting for transfers between devices: 151 us -> 102 us  [shards(): lax.all_gather(w_gate, 'sp', axis=1, tiled=True)]
    concatenate x0 -> x2, other arithmetic: none -> 12.6 us  [connect_sizes(): jnp.roll(jnp.concatenate(windows[::-1], 1), (lax.axis_index('tp') + 1) *...]
  transfers between devices with their start and end apart: 9 -> 13, of which waited for: 9 -> 13; matrix products, arithmetic and copies ran while one was open for 2% -> 3% of each run, Pallas kernels for 0% -> 0%
where the time goes in v1:
time: 626 us; the launch traced here: 625 us
  waiting for transfers between devices  526 us (84%)
  matrix products  31.8 us (5%)
  blocking collectives  26.3 us (4%)
  other arithmetic  19.1 us (3%)
  between operations  13.5 us (2%)
    all_gather x1, waiting for transfers between devices, shards(): lax.all_gather(w_value, 'sp', axis=1, tiled=True)  144 us
    all_gather x1, waiting for transfers between devices, shards(): out_all = lax.all_gather(w_out, 'sp', axis=2, tiled=True)  131 us
    all_gather x1, waiting for transfers between devices, shards(): lax.all_gather(w_gate, 'sp', axis=1, tiled=True)  102 us
    reduce_scatter x2, waiting for transfers between devices, shards(): lax.psum_scatter(partial_value.astype(jnp.bfloat16), 'tp', scatter_dimens...  75 us
    ppermute x6, waiting for transfers between devices, connect_sizes(): lax.ppermute(windows[-1], axis_name='tp', perm=[(rr, (rr + 1) % sides) fo...  68.5 us
    psum x2, blocking collectives, shards(): squares = lax.psum(jnp.sum(widened * widened, axis=1), 'tp')  14.1 us
    concatenate x2, other arithmetic, connect_sizes(): jnp.roll(jnp.concatenate(windows[::-1], 1), (lax.axis_index('tp') + 1) *...  12.6 us
  transfers between devices with their start and end apart: 13, of which 13 were waited for; matrix products, arithmetic and copies ran while one was open for 3% of the time, Pallas kernels for 0%

profile of v1, /device:TPU:0, one launch (start us, length us, event | category | flops | bytes accessed | tf_op | source)
XLA Modules:
  0.0 625.5 jit_solution(3969366722602050028)
XLA Ops:
  6.5 0.7 all-gather.6.cloned.1.call-update
  7.3 0.7 all-gather.4.cloned.1.call-update
  8.1 0.7 all-gather.8.cloned.1.call-update
  8.8 0.2 fusion.18
  9.0 8.4 %psum.42 = f32[384]{0:T(512)S(1)} all-reduce(f32[384]{0:T(512)S(1)} %fusion.18), channel_id=1, replica_groups=mesh['grp'=2,'sp'=4,'tp'=4] {'tp'}, use_global_device_ids=true, to_apply=%region_1.0 | all-reduce | flops 384 | bytes 3072 | tf_op jit(solution)/shard_map/psum | solution.py:56
  17.4 0.2 fusion.20
  17.7 11.4 %collective-permute-done = bf16[384,1024]{1,0:T(8,128)(2,1)S(1)} collective-permute-done((bf16[384,1024]{1,0:T(8,128)(2,1)S(1)}, bf16[384,1024]{1,0:T(8,128)(2,1)S(1)}, u32[]{:S(2)}, u32[]{:S(2)}) %collective-permute-start) | collective-permute-done | bytes 786464 | tf_op jit(solution)/shard_map/ppermute | solution.py:16
  29.1 11.4 %collective-permute-done.1 = bf16[384,1024]{1,0:T(8,128)(2,1)S(1)} collective-permute-done((bf16[384,1024]{1,0:T(8,128)(2,1)S(1)}, bf16[384,1024]{1,0:T(8,128)(2,1)S(1)}, u32[]{:S(2)}, u32[]{:S(2)}) %collective-permute-start.1) | collective-permute-done | bytes 786464 | tf_op jit(solution)/shard_map/ppermute | solution.py:16
  40.6 11.5 %collective-permute-done.2 = bf16[384,1024]{1,0:T(8,128)(2,1)} collective-permute-done((bf16[384,1024]{1,0:T(8,128)(2,1)S(1)}, bf16[384,1024]{1,0:T(8,128)(2,1)}, u32[]{:S(2)}, u32[]{:S(2)}) %collective-permute-start.2) | collective-permute-done | bytes 786464 | tf_op jit(solution)/shard_map/ppermute | solution.py:16
  52.1 7.2 %fusion.14 = bf16[384,4096]{1,0:T(8,128)(2,1)} fusion(s32[]{:T(128)S(6)} %select_n.13, bf16[384,1024]{1,0:T(8,128)(2,1)} %collective-permute-done.2, bf16[384,1024]{1,0:T(8,128)(2,1)S(1)} %collective-permute-done.1, bf16[384,1024]{1,0:T(8,128)(2,1)S(1)} %collective-permute-done, bf16[384,1024]{1,0:T(8,128)(2,1)S(1)} %fusion.20), kind=kLoop, calls=%fused_computation.38 | loop fusion | flops 25165824 | bytes 6291460 | tf_op jit(solution)/shard_map/jit(_roll_dynamic)/concatenate | solution.py:20
  59.3 102.0 %all-gather.6.cloned.1.call-done = bf16[2,4096,512]{2,1,0:T(8,128)(2,1)} async-done(((bf16[2,1024,512]{2,1,0:T(8,128)(2,1)}), bf16[2,4096,512]{2,1,0:T(8,128)(2,1)}) %all-gather.6.cloned.1.call-update) | async-done | bytes 8388624 | tf_op jit(solution)/shard_map/all_gather | solution.py:50
  161.3 5.0 fusion.37
  166.4 144.3 %all-gather.4.cloned.1.call-done = bf16[2,4096,512]{2,1,0:T(8,128)(2,1)} async-done(((bf16[2,1024,512]{2,1,0:T(8,128)(2,1)}), bf16[2,4096,512]{2,1,0:T(8,128)(2,1)}) %all-gather.4.cloned.1.call-update) | async-done | bytes 8388624 | tf_op jit(solution)/shard_map/all_gather | solution.py:49
  310.7 4.9 fusion.39
  315.6 1.3 collective-permute-start.3
  317.0 1.6 collective-permute-done.3
  318.5 0.1 maximum_bitcast_fusion
  318.7 0.1 copy.14
  319.0 1.9 fusion.79
  320.8 0.5 copy.16
  321.4 0.5 copy.15
  322.0 0.2 slice_reduce_fusion.1
  322.2 6.6 %all-reduce.1 = (f32[384]{0:T(512)S(1)}, f32[384]{0:T(512)S(1)}) all-reduce(f32[384]{0:T(512)S(1)} %get-tuple-element.24, f32[384]{0:T(512)S(1)} %get-tuple-element.25), channel_id=1, replica_groups=mesh['grp'=2,'sp'=4,'tp'=4] {'tp'}, use_global_device_ids=true, to_apply=%region_5.7 | all-reduce | flops 768 | bytes 6144 | tf_op jit(solution)/shard_map/psum | solution.py:68
  328.8 131.3 %all-gather.8.cloned.1.call-done = bf16[2,512,4096]{2,1,0:T(8,128)(2,1)} async-done(((bf16[2,512,1024]{2,1,0:T(8,128)(2,1)}), bf16[2,512,4096]{2,1,0:T(8,128)(2,1)}) %all-gather.8.cloned.1.call-update) | async-done | bytes 8388624 | tf_op jit(solution)/shard_map/all_gather | solution.py:52
  460.1 5.9 convolution_convert_fusion.1
  466.0 0.2 reduce-scatter.5.cloned.1.call-start
  466.2 35.8 %reduce-scatter.3.cloned.1.call-done = bf16[384,1024]{1,0:T(8,128)(2,1)} async-done(((bf16[384,4096]{1,0:T(8,128)(2,1)}), bf16[384,1024]{1,0:T(8,128)(2,1)}) %reduce-scatter.3.cloned.1.call-update) | async-done | bytes 786448 | tf_op jit(solution)/shard_map/reduce_scatter | solution.py:78
  502.0 1.5 fusion.22
  503.5 5.8 psum.45
  509.3 1.4 fusion.24
  510.8 11.4 %collective-permute-done.4 = bf16[384,1024]{1,0:T(8,128)(2,1)S(1)} collective-permute-done((bf16[384,1024]{1,0:T(8,128)(2,1)S(1)}, bf16[384,1024]{1,0:T(8,128)(2,1)S(1)}, u32[]{:S(2)}, u32[]{:S(2)}) %collective-permute-start.4) | collective-permute-done | bytes 786464 | tf_op jit(solution)/shard_map/ppermute | solution.py:16
  522.2 11.4 %collective-permute-done.5 = bf16[384,1024]{1,0:T(8,128)(2,1)S(1)} collective-permute-done((bf16[384,1024]{1,0:T(8,128)(2,1)S(1)}, bf16[384,1024]{1,0:T(8,128)(2,1)S(1)}, u32[]{:S(2)}, u32[]{:S(2)}) %collective-permute-start.5) | collective-permute-done | bytes 786464 | tf_op jit(solution)/shard_map/ppermute | solution.py:16
  533.6 11.4 %collective-permute-done.6 = bf16[384,1024]{1,0:T(8,128)(2,1)S(1)} collective-permute-done((bf16[384,1024]{1,0:T(8,128)(2,1)S(1)}, bf16[384,1024]{1,0:T(8,128)(2,1)S(1)}, u32[]{:S(2)}, u32[]{:S(2)}) %collective-permute-start.6) | collective-permute-done | bytes 786464 | tf_op jit(solution)/shard_map/ppermute | solution.py:16
  545.0 5.4 fusion.7
  550.4 4.3 fusion.35
  554.7 1.8 fusion.38
  556.5 3.6 collective-permute-start.7
  560.1 1.6 collective-permute-done.7
  561.9 0.1 copy.18
  562.2 2.0 fusion.80
  564.2 0.5 copy.20
  564.8 0.1 slice_reduce_fusion
  564.9 0.5 copy.19
  565.5 0.1 slice_reduce_fusion.2
  565.7 5.7 all-reduce
  571.4 6.0 convolution_convert_fusion
  577.3 39.2 %reduce-scatter.5.cloned.1.call-done = bf16[384,1024]{1,0:T(8,128)(2,1)} async-done(((bf16[384,4096]{1,0:T(8,128)(2,1)}), bf16[384,1024]{1,0:T(8,128)(2,1)}) %reduce-scatter.5.cloned.1.call-update) | async-done | bytes 786448 | tf_op jit(solution)/shard_map/reduce_scatter | solution.py:78
  616.5 2.4 fusion.25
  (53 shorter events, 1.2 us)
Async XLA Ops:
  6.5 2.3 copy-start
  6.5 10.9 %copy-start.2 = (f32[2,1024]{1,0:T(2,128)S(1)}, f32[2,1024]{1,0:T(2,128)}, u32[]{:S(2)}) copy-start(f32[2,1024]{1,0:T(2,128)} %param.11) | copy-start | bytes 24580
  6.5 34.0 %copy-start.3 = (f32[2,512]{1,0:T(2,128)S(1)}, f32[2,512]{1,0:T(2,128)}, u32[]{:S(2)}) copy-start(f32[2,512]{1,0:T(2,128)} %param.15) | copy-start | bytes 12292
  6.5 154.7 %all-gather.6.cloned.1.call-start = ((), (), s32[]{:S(2)}) async-start(), calls=%async_computation.3 | async-start | bytes 10485760 | tf_op jit(solution)/shard_map/all_gather | solution.py:50
  7.3 303.4 %all-gather.4.cloned.1.call-start = ((), (), s32[]{:S(2)}) async-start(), calls=%async_computation.2 | async-start | bytes 10485760 | tf_op jit(solution)/shard_map/all_gather | solution.py:49
  8.0 452.1 %all-gather.8.cloned.1.call-start = ((), (), s32[]{:S(2)}) async-start(), calls=%async_computation.4 | async-start | bytes 10485760 | tf_op jit(solution)/shard_map/all_gather | solution.py:52
  8.7 493.3 %reduce-scatter.3.cloned.1.call-start = ((), (), s32[]{:S(2)}) async-start(), calls=%async_computation.5 | async-start | bytes 3932160 | tf_op jit(solution)/shard_map/reduce_scatter | solution.py:78
  17.7 11.5 %collective-permute-start = (bf16[384,1024]{1,0:T(8,128)(2,1)S(1)}, bf16[384,1024]{1,0:T(8,128)(2,1)S(1)}, u32[]{:S(2)}, u32[]{:S(2)}) collective-permute-start(bf16[384,1024]{1,0:T(8,128)(2,1)S(1)} %fusion.20), channel_id=1, source_target_pairs={{0,1},{1,2},{2,3},{3,0},{4,5},{5,6},{6,7},{7,4},{8,9},{9,10},{10,1... | collective-permute-start | bytes 2359304 | tf_op jit(solution)/shard_map/ppermute | solution.py:16
  29.1 11.4 %collective-permute-start.1 = (bf16[384,1024]{1,0:T(8,128)(2,1)S(1)}, bf16[384,1024]{1,0:T(8,128)(2,1)S(1)}, u32[]{:S(2)}, u32[]{:S(2)}) collective-permute-start(bf16[384,1024]{1,0:T(8,128)(2,1)S(1)} %collective-permute-done), channel_id=1, source_target_pairs={{0,1},{1,2},{2,3},{3,0},{4,5},{5,6},{6,7},{7,4},{8,9},{9,10},{10,1... | collective-permute-start | bytes 2359304 | tf_op jit(solution)/shard_map/ppermute | solution.py:16
  40.6 11.5 %collective-permute-start.2 = (bf16[384,1024]{1,0:T(8,128)(2,1)S(1)}, bf16[384,1024]{1,0:T(8,128)(2,1)}, u32[]{:S(2)}, u32[]{:S(2)}) collective-permute-start(bf16[384,1024]{1,0:T(8,128)(2,1)S(1)} %collective-permute-done.1), channel_id=1, source_target_pairs={{0,1},{1,2},{2,3},{3,0},{4,5},{5,6},{6,7},{7,4},{8,9},{9,10},{10,1... | collective-permute-start | bytes 2359304 | tf_op jit(solution)/shard_map/ppermute | solution.py:16
  166.3 150.6 %copy-start.4 = (f32[2,512]{1,0:T(2,128)S(1)}, f32[2,512]{1,0:T(2,128)}, u32[]{:S(2)}) copy-start(f32[2,512]{1,0:T(2,128)} %param.16) | copy-start | bytes 12292
  166.3 152.6 %copy-start.5 = (f32[2,31,512]{2,0,1:T(2,128)S(1)}, f32[2,31,512]{2,0,1:T(2,128)}, u32[]{:S(2)}) copy-start(f32[2,31,512]{2,0,1:T(2,128)} %param.14) | copy-start | bytes 380932
  166.3 152.6 %copy-start.6 = (pred[8,52]{0,1:T(8,128)(4,1)S(1)}, pred[8,52]{0,1:T(8,128)(4,1)}, u32[]{:S(2)}) copy-start(pred[8,52]{0,1:T(8,128)(4,1)} %constant.56) | copy-start | bytes 1252
  315.6 2.9 collective-permute-start.3
  466.0 150.5 %reduce-scatter.5.cloned.1.call-start = ((), (), s32[]{:S(2)}) async-start(), calls=%async_computation.6 | async-start | bytes 3932160 | tf_op jit(solution)/shard_map/reduce_scatter | solution.py:78
  510.7 11.5 %collective-permute-start.4 = (bf16[384,1024]{1,0:T(8,128)(2,1)S(1)}, bf16[384,1024]{1,0:T(8,128)(2,1)S(1)}, u32[]{:S(2)}, u32[]{:S(2)}) collective-permute-start(bf16[384,1024]{1,0:T(8,128)(2,1)S(1)} %fusion.24), channel_id=1, source_target_pairs={{0,1},{1,2},{2,3},{3,0},{4,5},{5,6},{6,7},{7,4},{8,9},{9,10},{10,1... | collective-permute-start | bytes 2359304 | tf_op jit(solution)/shard_map/ppermute | solution.py:16
  522.2 11.4 %collective-permute-start.5 = (bf16[384,1024]{1,0:T(8,128)(2,1)S(1)}, bf16[384,1024]{1,0:T(8,128)(2,1)S(1)}, u32[]{:S(2)}, u32[]{:S(2)}) collective-permute-start(bf16[384,1024]{1,0:T(8,128)(2,1)S(1)} %collective-permute-done.4), channel_id=1, source_target_pairs={{0,1},{1,2},{2,3},{3,0},{4,5},{5,6},{6,7},{7,4},{8,9},{9,10},{10,1... | collective-permute-start | bytes 2359304 | tf_op jit(solution)/shard_map/ppermute | solution.py:16
  533.6 11.4 %collective-permute-start.6 = (bf16[384,1024]{1,0:T(8,128)(2,1)S(1)}, bf16[384,1024]{1,0:T(8,128)(2,1)S(1)}, u32[]{:S(2)}, u32[]{:S(2)}) collective-permute-start(bf16[384,1024]{1,0:T(8,128)(2,1)S(1)} %collective-permute-done.5), channel_id=1, source_target_pairs={{0,1},{1,2},{2,3},{3,0},{4,5},{5,6},{6,7},{7,4},{8,9},{9,10},{10,1... | collective-permute-start | bytes 2359304 | tf_op jit(solution)/shard_map/ppermute | solution.py:16
  545.0 9.7 %slice-start = ((s8[8388608]{0:T(1024)(128)(4,1)}), s8[4194304]{0:T(1024)(128)(4,1)S(1)}, s32[]{:S(2)}) async-start(s8[8388608]{0:T(1024)(128)(4,1)} %bitcast.88), calls=%async_computation.7 | async-start | bytes 8388608
  550.4 4.3 slice-start.1
  554.7 7.4 %copy-start.7 = (pred[8,52]{0,1:T(8,128)(4,1)S(1)}, pred[8,52]{0,1:T(8,128)(4,1)}, u32[]{:S(2)}) copy-start(pred[8,52]{0,1:T(8,128)(4,1)} %constant.56) | copy-start | bytes 1252
  556.5 5.2 collective-permute-start.7
  571.3 45.2 %copy-start.1 = (bf16[384,1024]{1,0:T(8,128)(2,1)S(1)}, bf16[384,1024]{1,0:T(8,128)(2,1)}, u32[]{:S(2)}) copy-start(bf16[384,1024]{1,0:T(8,128)(2,1)} %reduce-scatter.3.cloned.1.call-done) | copy-start | bytes 2359300
Sparse Core Ops, SparseCore 0:
  8.9 152.3 all-gather.5
  162.8 147.7 all-gather.3
  312.3 147.7 all-gather.7
  466.1 35.8 reduce-scatter.2
  577.5 38.9 reduce-scatter.4
